TPU v7x, 32 devices: a whole 2x2x4 slice. The times are simulated.
32 devices in a mesh: rep: 2 (over core), fs: 8 (over z, y), tp: 2 (over x).
Axes of the slice: x: 2, y: 2, z: 4, core: 2. Of those that a mesh axis runs over, the one named last changes fastest.
Arguments:
- resid: bfloat16 [16, 1024, 2048], P(('rep', 'fs')), may hold values from -6 to 6
- attention_norm_gain: float32 [2048], replicated, may hold values from 0.1 to 1.9
- query_weight: bfloat16 [2048, 1024], P('fs', 'tp'), may hold values from -0.125 to 0.125
- key_weight: bfloat16 [2048, 1024], P('fs', 'tp'), may hold values from -0.125 to 0.125
- value_weight: bfloat16 [2048, 2048], P('fs', 'tp'), may hold values from -0.125 to 0.125
- decay_down_weight: bfloat16 [2048, 16], replicated, may hold values from -0.125 to 0.125
- decay_up_weight: bfloat16 [16, 1024], replicated, may hold values from -1.5 to 1.5
- decay_rate_bias: float32 [1024], replicated, may hold values from 0.3 to 7
- decay_increment: float32 [16, 1024, 8], P(('rep', 'fs'), None, 'tp'), may hold values from -0.7 to 0, as said below
- head_norm_gain: float32 [256], replicated, may hold values from 0.1 to 1.9
- feedforward_norm_gain: float32 [2048], replicated, may hold values from 0.1 to 1.9
- up_weight: bfloat16 [2048, 4096], P('fs', 'tp'), may hold values from -0.125 to 0.125
- down_weight: bfloat16 [4096, 2048], P('tp', 'fs'), may hold values from -0.09375 to 0.09375
Outputs:
- layer_out: bfloat16 [16, 1024, 2048], P(('rep', 'fs'), None, 'tp')
Inputs may be any that keep to these rules, and one draw needn't show every extreme that they name: `decay_increment`: each entry is zero or a negative log-decay.
All inputs are finite; a program needn't handle non-finite values.
Results may differ from a plain program's by a relative error of at most 0.014.
Values may be sent and summed in bfloat16 or wider, within the bound.
A program may use at most 64 MiB of HBM per device.

v0:
```python
import jax
import jax.numpy as jnp
from jax import lax
from jax.sharding import PartitionSpec as P

KEY_CHANNELS = 128
HEAD_V = 256
BLOCK = 64


EPS = 1e-06
HIGH = lax.Precision.HIGHEST


def rms_rows(rows_in, gain_vec):
    values_f = rows_in.astype(jnp.float32)
    scaled = values_f * lax.rsqrt(jnp.mean(values_f * values_f, axis=-1, keepdims=True) + EPS)
    return (scaled * gain_vec).astype(jnp.bfloat16)


def head_major(product, head_width):
    rounded = lax.optimization_barrier(product.astype(jnp.bfloat16)).astype(jnp.float32)
    return rounded.reshape(product.shape[0], -1, head_width).transpose(1, 0, 2)


def gated_scan(queries, keys_in, values_in, logarithm_decay_rates):
    head_count, sequence_length, key_width = queries.shape
    value_width = values_in.shape[-1]
    blocks = sequence_length // BLOCK

    def split_blocks(source):
        return source.reshape(head_count, blocks, BLOCK, source.shape[-1]).transpose(1, 0, 2, 3)

    causal_mask = jnp.tril(jnp.ones((BLOCK, BLOCK), dtype=bool))

    def block_step(carry_state, input_tokens):
        q_blk, k_blk, v_blk, g_blk = input_tokens
        cumulative = jnp.cumsum(g_blk, axis=1)
        carried = jnp.einsum(
            "hcd,hde->hce", q_blk * jnp.exp(cumulative), carry_state, precision=HIGH
        )
        log_gaps = cumulative[:, :, None, :] - cumulative[:, None, :, :]
        decays = jnp.exp(jnp.where(causal_mask[None, :, :, None], log_gaps, -jnp.inf))
        scores = jnp.sum(q_blk[:, :, None, :] * k_blk[:, None, :, :] * decays, axis=-1)
        outputs = carried + jnp.einsum("hij,hje->hie", scores, v_blk, precision=HIGH)
        last_cum = cumulative[:, -1:, :]
        new_state = jnp.exp(last_cum[:, 0, :])[:, :, None] * carry_state + jnp.einsum(
            "hcd,hce->hde", k_blk * jnp.exp(last_cum - cumulative), v_blk, precision=HIGH
        )
        return (new_state, outputs)

    start_state = jnp.zeros((head_count, key_width, value_width), jnp.float32)
    final_state, outputs = lax.scan(
        block_step,
        start_state,
        (
            split_blocks(queries),
            split_blocks(keys_in),
            split_blocks(values_in),
            split_blocks(logarithm_decay_rates),
        ),
    )
    return outputs.transpose(1, 0, 2, 3).reshape(head_count, sequence_length, value_width)


def column_adder(source, portions):
    return tuple(
        (jnp.dot(source, portion, preferred_element_type=jnp.float32) for portion in portions)
    )


def per_device(
    resid,
    attention_norm_gain,
    query_weight,
    key_weight,
    value_weight,
    decay_down_weight,
    decay_up_weight,
    decay_rate_bias,
    decay_increment,
    head_norm_gain,
    feedforward_norm_gain,
    up_weight,
    down_weight,
):
    sequence_rows = resid[0]
    sequence_length = sequence_rows.shape[0]
    col_width = value_weight.shape[1]
    col_start = lax.axis_index("tp") * col_width
    own_cols = lax.dynamic_slice_in_dim(sequence_rows, col_start, col_width, 1)
    down_full = lax.all_gather(down_weight, "fs", axis=1, tiled=True)
    normed = rms_rows(sequence_rows, attention_norm_gain)
    width_qk = query_weight.shape[1]
    query_acc, key_acc, value_acc = column_adder(
        normed,
        (
            lax.all_gather(query_weight, "fs", axis=0, tiled=True),
            lax.all_gather(key_weight, "fs", axis=0, tiled=True),
            lax.all_gather(value_weight, "fs", axis=0, tiled=True),
        ),
    )
    head_here = width_qk // KEY_CHANNELS
    first_col = lax.axis_index("tp") * width_qk
    rate_cols = lax.dynamic_slice_in_dim(decay_up_weight, first_col, width_qk, 1)
    bias_cols = lax.dynamic_slice_in_dim(decay_rate_bias, first_col, width_qk, 0)
    rate_low = jnp.dot(normed, decay_down_weight, preferred_element_type=jnp.float32).astype(
        jnp.bfloat16
    )
    decay_rate_logits = jnp.dot(rate_low, rate_cols, preferred_element_type=jnp.float32) + bias_cols
    logarithm_decay_rates = (jax.nn.log_sigmoid(decay_rate_logits) / 16.0).reshape(
        sequence_length, head_here, KEY_CHANNELS
    ) + decay_increment[0][:, :, None]
    queries = head_major(query_acc, KEY_CHANNELS) * KEY_CHANNELS ** (-0.5)
    keys_in = head_major(key_acc, KEY_CHANNELS)
    values_in = head_major(value_acc, HEAD_V)
    head_out = gated_scan(queries, keys_in, values_in, logarithm_decay_rates.transpose(1, 0, 2))
    normalized = (
        head_out
        * lax.rsqrt(jnp.mean(head_out * head_out, axis=-1, keepdims=True) + EPS)
        * head_norm_gain
    )
    flat = normalized.transpose(1, 0, 2).reshape(sequence_length, col_width)
    middle_cols = (own_cols.astype(jnp.float32) + flat).astype(jnp.bfloat16)
    middle_all = lax.all_gather(middle_cols, "tp", axis=1, tiled=True)
    normed_mlp = rms_rows(middle_all, feedforward_norm_gain)
    up_acc = column_adder(normed_mlp, (lax.all_gather(up_weight, "fs", axis=0, tiled=True),))[0]
    hidden = jnp.square(jax.nn.relu(up_acc)).astype(jnp.bfloat16)
    terms = jnp.dot(hidden, down_full, preferred_element_type=jnp.float32)
    summed = lax.psum_scatter(
        terms.astype(jnp.bfloat16), "tp", scatter_dimension=1, tiled=True
    ).astype(jnp.float32)
    out_cols = (middle_cols.astype(jnp.float32) + summed).astype(jnp.bfloat16)
    return out_cols[None]


def solution(mesh):
    return jax.shard_map(
        per_device,
        mesh=mesh,
        in_specs=(
            P(("rep", "fs"), None, None),
            P(),
            P("fs", "tp"),
            P("fs", "tp"),
            P("fs", "tp"),
            P(),
            P(),
            P(),
            P(("rep", "fs"), None, "tp"),
            P(),
            P(),
            P("fs", "tp"),
            P("tp", "fs"),
        ),
        out_specs=P(("rep", "fs"), None, "tp"),
        check_vma=False,
    )
```

profile of v0, /device:TPU:0, one launch (start us, length us, event | category | flops | bytes accessed | tf_op | source)
XLA Modules:
  0.0 760.6 jit_solution(17804629656650264291)
XLA Ops:
  9.6 3.1 fusion.24
  12.7 6.1 fusion.44
  18.8 2.0 copy.24
  20.8 1.9 broadcast_add_fusion
  22.8 38.5 %all-gather.7.cloned.1.call-done = bf16[2048,512]{1,0:T(8,128)(2,1)} async-done(((bf16[256,512]{1,0:T(8,128)(2,1)}), bf16[2048,512]{1,0:T(8,128)(2,1)}) %all-gather.7.cloned.1.call-update) | async-done | bytes 2097168 | tf_op jit(solution)/shard_map/all_gather | solution.py:99
  61.3 6.3 convolution_convert_fusion.2
  67.6 43.5 %all-gather.11.cloned.1.call-done = bf16[2048,512]{1,0:T(8,128)(2,1)} async-done(((bf16[256,512]{1,0:T(8,128)(2,1)}), bf16[2048,512]{1,0:T(8,128)(2,1)}) %all-gather.11.cloned.1.call-update) | async-done | bytes 2097168 | tf_op jit(solution)/shard_map/all_gather | solution.py:98
  111.1 5.3 convolution_convert_fusion.1
  118.1 66.5 %all-gather.9.cloned.1.call-done = bf16[2048,1024]{1,0:T(8,128)(2,1)} async-done(((bf16[256,1024]{1,0:T(8,128)(2,1)}), bf16[2048,1024]{1,0:T(8,128)(2,1)}) %all-gather.9.cloned.1.call-update) | async-done | bytes 4194320 | tf_op jit(solution)/shard_map/all_gather | solution.py:100
  184.6 8.0 %convolution_convert_fusion = bf16[1024,1024]{1,0:T(8,128)(2,1)S(1)} fusion(bf16[2048,1024]{1,0:T(8,128)(2,1)} %all-gather.9.cloned.1.call-done, bf16[1,1024,2048]{2,1,0:T(8,128)(2,1)} %param.15, f32[2048]{0:T(1024)S(1)} %copy-done.8, f32[1024]{0:T(1024)S(1)} %add_rsqrt_fusion.2), kind=kOutput, calls=%fused_computation.59 | convolution fusion | flops 4304404480 | bytes 10498048 | tf_op jit(solution)/shard_map/dot_general | solution.py:68
  193.0 2.4 copy.50
  195.4 159.3 %while.13 = (s32[]{:T(128)}, f32[4,128,256]{2,1,0:T(8,128)S(1)}, f32[16,4,64,256]{3,2,0,1:T(8,128)}, f32[16,4,64,128]{3,2,0,1:T(8,128)}, f32[16,4,64,128]{3,2,0,...) while((s32[]{:T(128)}, f32[4,128,256]{2,1,0:T(8,128)S(1)}, ...), condition=%wide.region_4.5_spmd.clone, body=%wide.region_1.4_spmd.clone.sunk | while | flops 264884224 | bytes 5003388 | solution.py:53
  197.4 3.7 multiply_reduce_fusion.2
  201.6 2.0 fusion.75
  207.4 3.7 multiply_reduce_fusion.2
  211.6 2.0 fusion.75
  213.6 1.7 convolution_add_fusion.3
  217.3 3.7 multiply_reduce_fusion.2
  221.5 2.0 fusion.75
  223.5 1.7 convolution_add_fusion.3
  227.2 3.7 multiply_reduce_fusion.2
  231.4 2.0 fusion.75
  237.2 3.7 multiply_reduce_fusion.2
  241.4 2.0 fusion.75
  247.1 3.7 multiply_reduce_fusion.2
  251.3 2.0 fusion.75
  257.0 3.7 multiply_reduce_fusion.2
  261.2 2.0 fusion.75
  263.3 1.7 convolution_add_fusion.3
  267.0 3.7 multiply_reduce_fusion.2
  271.2 2.0 fusion.75
  273.2 1.7 convolution_add_fusion.3
  276.9 3.7 multiply_reduce_fusion.2
  281.1 2.0 fusion.75
  283.2 1.7 convolution_add_fusion.3
  286.9 3.7 multiply_reduce_fusion.2
  291.1 2.0 fusion.75
  293.1 1.7 convolution_add_fusion.3
  296.8 3.7 multiply_reduce_fusion.2
  301.0 2.0 fusion.75
  306.8 3.7 multiply_reduce_fusion.2
  311.0 2.0 fusion.75
  316.7 3.7 multiply_reduce_fusion.2
  320.9 2.0 fusion.75
  323.0 1.7 convolution_add_fusion.3
  326.6 3.7 multiply_reduce_fusion.2
  330.9 2.0 fusion.75
  332.9 1.7 convolution_add_fusion.3
  336.6 3.7 multiply_reduce_fusion.2
  340.8 2.0 fusion.75
  342.8 1.7 convolution_add_fusion.3
  346.5 3.7 multiply_reduce_fusion.2
  350.7 2.0 fusion.75
  354.7 2.8 fusion.33
  357.6 2.6 fusion.31
  360.8 1.7 copy-done.3
  362.4 2.1 fusion.32
  365.8 54.2 %all-gather.13.cloned.1.call-done = bf16[1024,2048]{1,0:T(8,128)(2,1)} async-done(((bf16[1024,1024]{1,0:T(8,128)(2,1)}), bf16[1024,2048]{1,0:T(8,128)(2,1)}) %all-gather.13.cloned.1.call-update) | async-done | bytes 4194320 | tf_op jit(solution)/shard_map/all_gather | solution.py:125
  420.0 3.1 fusion.21
  423.1 123.4 %all-gather.15.cloned.1.call-done = bf16[2048,2048]{1,0:T(8,128)(2,1)} async-done(((bf16[256,2048]{1,0:T(8,128)(2,1)}), bf16[2048,2048]{1,0:T(8,128)(2,1)}) %all-gather.15.cloned.1.call-update) | async-done | bytes 8388624 | tf_op jit(solution)/shard_map/all_gather | solution.py:127
  546.5 125.0 %all-gather.17.cloned.1.call-done = bf16[2048,2048]{1,0:T(8,128)(2,1)} async-done(((bf16[2048,256]{1,0:T(8,128)(2,1)}), bf16[2048,2048]{1,0:T(8,128)(2,1)}) %all-gather.17.cloned.1.call-update) | async-done | bytes 8388624 | tf_op jit(solution)/shard_map/all_gather | solution.py:92
  671.5 25.6 %fusion.39 = bf16[1024,2048]{1,0:T(8,128)(2,1)} fusion(bf16[2048,2048]{1,0:T(8,128)(2,1)} %all-gather.17.cloned.1.call-done, bf16[2048,2048]{1,0:T(8,128)(2,1)} %all-gather.15.cloned.1.call-done, bf16[1024,2048]{1,0:T(8,128)(2,1)} %all-gather.13.cloned.1.call-done, f32[2048]{0:T(1024)S(1)} %copy-done.9, f32[1024]{0:T(1024)S(1)} %add_rsqrt_fusion.1), kind=kOutput, calls=%fused_computation.51 | convolution fusion | flops 17196646400 | bytes 25178112 | tf_op jit(solution)/shard_map/dot_general | solution.py:129
  697.2 52.7 %reduce-scatter.2.cloned.1.call-done = bf16[1024,1024]{1,0:T(8,128)(2,1)} async-done(((bf16[1024,2048]{1,0:T(8,128)(2,1)}), bf16[1024,1024]{1,0:T(8,128)(2,1)}) %reduce-scatter.2.cloned.1.call-update) | async-done | bytes 2097168 | tf_op jit(solution)/shard_map/reduce_scatter | solution.py:130
  749.9 3.9 fusion.42
  (163 shorter events, 58.0 us)
Async XLA Ops:
  6.5 6.1 copy-start
  6.5 6.1 copy-start.8
  6.5 6.2 copy-start.7
  6.5 54.8 %all-gather.7.cloned.1.call-start = ((), (), s32[]{:S(2)}) async-start(), calls=%async_computation.1 | async-start | bytes 2359296 | tf_op jit(solution)/shard_map/all_gather | solution.py:99
  7.3 103.8 %all-gather.11.cloned.1.call-start = ((), (), s32[]{:S(2)}) async-start(), calls=%async_computation.3 | async-start | bytes 2359296 | tf_op jit(solution)/shard_map/all_gather | solution.py:98
  8.0 176.6 %all-gather.9.cloned.1.call-start = ((), (), s32[]{:S(2)}) async-start(), calls=%async_computation.2 | async-start | bytes 4718592 | tf_op jit(solution)/shard_map/all_gather | solution.py:100
  8.7 411.2 %all-gather.13.cloned.1.call-start = ((), (), s32[]{:S(2)}) async-start(), calls=%async_computation.4 | async-start | bytes 6291456 | tf_op jit(solution)/shard_map/all_gather | solution.py:125
  18.8 2.0 copy-start.5
  111.1 5.3 copy-start.4
  354.7 2.9 copy-start.6
  360.2 2.2 copy-start.3
  364.6 307.0 %copy-start.9 = (f32[2048]{0:T(1024)S(1)}, f32[2048]{0:T(1024)}, u32[]{:S(2)}) copy-start(f32[2048]{0:T(1024)} %param.25) | copy-start | bytes 24580
  364.6 181.9 %all-gather.15.cloned.1.call-start = ((), (), s32[]{:S(2)}) async-start(), calls=%async_computation.5 | async-start | bytes 9437184 | tf_op jit(solution)/shard_map/all_gather | solution.py:127
  365.2 306.3 %all-gather.17.cloned.1.call-start = ((), (), s32[]{:S(2)}) async-start(), calls=%async_computation.6 | async-start | bytes 9437184 | tf_op jit(solution)/shard_map/all_gather | solution.py:92
  365.8 384.2 %reduce-scatter.2.cloned.1.call-start = ((), (), s32[]{:S(2)}) async-start(), calls=%async_computation.7 | async-start | bytes 6291456 | tf_op jit(solution)/shard_map/reduce_scatter | solution.py:130
  697.1 52.8 %copy-start.2 = (bf16[1024,1024]{1,0:T(8,128)(2,1)S(1)}, bf16[1024,1024]{1,0:T(8,128)(2,1)}, u32[]{:S(2)}) copy-start(bf16[1024,1024]{1,0:T(8,128)(2,1)} %fusion.32) | copy-start | bytes 6291460
  697.2 56.6 %copy-start.1 = (bf16[2048,16]{0,1:T(8,128)(2,1)S(1)}, bf16[2048,16]{0,1:T(8,128)(2,1)}, u32[]{:S(2)}) copy-start(bf16[2048,16]{0,1:T(8,128)(2,1)} %param.20) | copy-start | bytes 196612
Sparse Core Ops, SparseCore 0:
  9.5 51.7 all-gather.6
  63.4 47.6 all-gather.10
  113.2 71.3 all-gather.8
  364.7 55.2 all-gather.12
  422.0 124.4 all-gather.14
  548.4 123.1 all-gather.16
  697.3 52.5 reduce-scatter.1
where the time goes:
time: 763 us; the launch traced here: 761 us
  waiting for transfers between devices  507 us (66%)
  matrix products  117 us (15%)
  other arithmetic  83.9 us (11%)
  local copies, waits for them, and re-layouts  37.3 us (5%)
  between operations  13.7 us (2%)
    all_gather x1, waiting for transfers between devices, per_device(): down_full = lax.all_gather(down_weight, 'fs', axis=1, tiled=True)  125 us
    all_gather x1, waiting for transfers between devices, per_device(): lax.all_gather(up_weight, 'fs', axis=0, tiled=True)  123 us
    all_gather x1, waiting for transfers between devices, per_device(): lax.all_gather(value_weight, 'fs', axis=0, tiled=True)  66.5 us
    reduce_sum x16, other arithmetic, block_step(): jnp.sum(q_blk[:, :, None, :] * k_blk[:, None, :, :] * decays, axis=-1)  59.8 us
    all_gather x1, waiting for transfers between devices, per_device(): middle_all = lax.all_gather(middle_cols, 'tp', axis=1, tiled=True)  54.2 us
    reduce_scatter x1, waiting for transfers between devices, per_device(): lax.psum_scatter(terms.astype(jnp.bfloat16), 'tp', scatter_dimension=1, t...  52.7 us
    all_gather x1, waiting for transfers between devices, per_device(): lax.all_gather(query_weight, 'fs', axis=0, tiled=True)  43.5 us
    all_gather x1, waiting for transfers between devices, per_device(): lax.all_gather(key_weight, 'fs', axis=0, tiled=True)  38.5 us
  transfers between devices with their start and end apart: 7, of which 7 were waited for; matrix products, arithmetic and copies ran while one was open for 4% of the time, Pallas kernels for 0%

commit v1 on v0

v1 whole, which is shorter than its diff:
```python
import functools

import jax
import jax.numpy as jnp
import numpy as np
from jax import lax
from jax.experimental import pallas as pl
from jax.experimental.pallas import tpu as pltpu
from jax.sharding import PartitionSpec as P

KEY_CHANNELS = 128
HEAD_V = 256
BLOCK = 64
FINE = 8
STRIDE = 4
ROWS = 128


EPS = 1e-06
MESH = pl.DeviceIdType.MESH
VMEM_LIMIT = 60 * 1024 * 1024


def rms_rows(rows_in, gain_vec):
    values_f = rows_in.astype(jnp.float32)
    scaled = values_f * lax.rsqrt(jnp.mean(values_f * values_f, axis=-1, keepdims=True) + EPS)
    return (scaled * gain_vec).astype(jnp.bfloat16)


def ring_to_fs(place, n):
    return jnp.where(place < n // 2, 2 * place, 2 * (n - 1 - place) + 1)


def fs_to_ring(fs, n):
    return jnp.where(lax.rem(fs, 2) == 0, fs // 2, n - 1 - fs // 2)


class Ring:
    def __init__(self, n, shards, held, full, sems):
        self.n, self.hops = n, n // 2
        self.shards, self.held, self.full = shards, held, full
        self.out_sem, self.in_sem, self.twin_out, self.twin_in, self.local = sems
        self.rep, self.fs, self.tp = (lax.axis_index(a) for a in ("rep", "fs", "tp"))
        self.me = fs_to_ring(self.fs, n)
        right = ring_to_fs(lax.rem(self.me + 1, n), n)
        left = ring_to_fs(lax.rem(self.me + n - 1, n), n)
        self.way_id = ((self.rep, right, self.tp), (self.rep, left, self.tp))
        self.twin_id = (1 - self.rep, self.fs, self.tp)

    def greet(self, others=()):
        barrier = pltpu.get_barrier_semaphore()
        who = (*self.way_id, self.twin_id, *others)
        for device in who:
            pl.semaphore_signal(barrier, inc=1, device_id=device, device_id_type=MESH)
        pl.semaphore_wait(barrier, len(who))

    def span(self, k, hop, way):
        half = self.held[k].shape[0] // 2
        source = ring_to_fs(lax.rem(self.me + (self.n - hop if way == 0 else hop), self.n), self.n)
        return source * (2 * half) + self.rep * half, half

    def cut(self, half, hop, way):
        if hop < self.hops - 1:
            return 0, half
        return (0, half // 2) if way == 0 else (half // 2, half - half // 2)

    def sending(self, k, hop, way):
        start, half = self.span(k, hop, way)
        shift, size = self.cut(half, hop, way)
        target = self.full[k].at[pl.ds(pl.multiple_of(start + shift, 16), size)]
        source = target
        if hop == 0:
            source = self.held[k].at[pl.ds(pl.multiple_of(self.rep * half + shift, 16), size)]
        return pltpu.make_async_remote_copy(
            src_ref=source,
            dst_ref=target,
            send_sem=self.out_sem.at[k, way, hop],
            recv_sem=self.in_sem.at[k, way, hop],
            device_id=self.way_id[way],
            device_id_type=MESH,
        )

    def landing(self, k, hop, way):
        start, half = self.span(k, hop + 1, way)
        shift, size = self.cut(half, hop, way)
        return self.full[k].at[pl.ds(pl.multiple_of(start + shift, 16), size)]

    def twin(self, k, hop, way):
        landed = self.landing(k, hop, way)
        return pltpu.make_async_remote_copy(
            src_ref=landed,
            dst_ref=landed,
            send_sem=self.twin_out.at[k, way, hop],
            recv_sem=self.twin_in.at[k, way, hop],
            device_id=self.twin_id,
            device_id_type=MESH,
        )

    def load(self, k):
        return pltpu.make_async_copy(self.shards[k], self.held[k], self.local.at[k, 0])

    def keep(self, k):
        rows = self.held[k].shape[0]
        at = pl.ds(pl.multiple_of(self.fs * rows, 16), rows)
        return pltpu.make_async_copy(self.held[k], self.full[k].at[at], self.local.at[k, 1])

    def start(self, others=()):
        count = len(self.held)
        for k in range(count):
            self.load(k).start()
        self.greet(others)
        for k in range(count):
            self.load(k).wait()
            for way in range(2):
                self.sending(k, 0, way).start()
        for k in range(count):
            self.keep(k).start()

    def events(self):
        return [(k, hop) for hop in range(self.hops) for k in range(len(self.held))]

    def event(self, k, hop):
        for way in range(2):
            landed = self.landing(k, hop, way)
            pltpu.make_async_remote_copy(
                src_ref=landed,
                dst_ref=landed,
                send_sem=self.out_sem.at[k, way, hop],
                recv_sem=self.in_sem.at[k, way, hop],
                device_id=self.way_id[way],
                device_id_type=MESH,
            ).wait_recv()
            if hop < self.hops - 1:
                self.sending(k, hop + 1, way).start()
            self.twin(k, hop, way).start()

    def finish(self):
        for k, hop in self.events():
            for way in range(2):
                self.sending(k, hop, way).wait_send()
                copy = self.twin(k, hop, way)
                copy.wait_send()
                start, half = self.span(k, hop + 1, way)
                other = start + (1 - 2 * self.rep) * half
                shift, size = self.cut(half, hop, way)
                there = self.full[k].at[pl.ds(pl.multiple_of(other + shift, 16), size)]
                pltpu.make_async_remote_copy(
                    src_ref=there,
                    dst_ref=there,
                    send_sem=self.twin_out.at[k, way, hop],
                    recv_sem=self.twin_in.at[k, way, hop],
                    device_id=self.twin_id,
                    device_id_type=MESH,
                ).wait_recv()
        for k in range(len(self.held)):
            self.keep(k).wait()


def ring_scratch(shards, n):
    count = len(shards)
    return [pltpu.VMEM(s.shape, s.dtype) for s in shards] + [
        pltpu.SemaphoreType.DMA((count, 2, n // 2)) for _ in range(4)
    ] + [pltpu.SemaphoreType.DMA((count, 2))]


def gathered_shapes(shards, n):
    return [jax.ShapeDtypeStruct((n * s.shape[0], s.shape[1]), s.dtype) for s in shards]


def gather_kernel(n, count, *refs):
    ring = Ring(n, refs[:count], refs[2 * count : 3 * count], refs[count : 2 * count], refs[3 * count :])
    ring.start()
    for k, hop in ring.events():
        ring.event(k, hop)
    ring.finish()


def ring_gather(shards, n, collective_id):
    count = len(shards)
    anywhere = pl.BlockSpec(memory_space=pl.ANY)
    return pl.pallas_call(
        functools.partial(gather_kernel, n, count),
        out_shape=gathered_shapes(shards, n),
        in_specs=[anywhere] * count,
        out_specs=[anywhere] * count,
        scratch_shapes=ring_scratch(shards, n),
        compiler_params=pltpu.CompilerParams(collective_id=collective_id, has_side_effects=True),
    )(*shards)


def decay_matrices():
    row = np.arange(BLOCK)[:, None]
    col = np.arange(BLOCK)[None, :]
    stack = [col <= row, col > row]
    half = BLOCK // 2
    while half >= FINE:
        ref = row // (2 * half) * (2 * half) + half - 1
        late = row % (2 * half) >= half
        stack.append(np.where(late, (col > ref) & (col <= row), (col > row) & (col <= ref)))
        half //= 2
    stack.append((col <= row) & (col // FINE == row // FINE))
    one = np.concatenate(stack, axis=0).astype(np.float32)
    return np.concatenate([one, one], axis=1)


def attention_block(
    heads,
    q_ref,
    k_ref,
    v_ref,
    low_ref,
    rate_ref,
    bias_ref,
    incr_ref,
    own_ref,
    gain_ref,
    sums_ref,
    spread_ref,
    out_ref,
    state,
):
    bf, f32 = jnp.bfloat16, jnp.float32
    logits = jnp.dot(low_ref[...], rate_ref[...], preferred_element_type=f32) + bias_ref[...]
    rates = (jnp.minimum(logits, 0.0) - jnp.log1p(jnp.exp(-jnp.abs(logits)))) * (1.0 / 16.0)
    increments = incr_ref[...]
    row = lax.broadcasted_iota(jnp.int32, (BLOCK, BLOCK), 0)
    col = lax.broadcasted_iota(jnp.int32, (BLOCK, BLOCK), 1)
    row_id = lax.broadcasted_iota(jnp.int32, (BLOCK, KEY_CHANNELS), 0)
    contract_last = (((1,), (1,)), ((), ()))
    for h in range(heads):
        keys_at = pl.ds(h * KEY_CHANNELS, KEY_CHANNELS)
        values_at = pl.ds(h * HEAD_V, HEAD_V)
        g = rates[:, h * KEY_CHANNELS : (h + 1) * KEY_CHANNELS] + increments[:, h : h + 1]
        high = g.astype(bf)
        low = (g - high.astype(f32)).astype(bf)
        sums = jnp.dot(
            sums_ref[...], jnp.concatenate([high, low], axis=0), preferred_element_type=f32
        )
        parts = [sums[i * BLOCK : (i + 1) * BLOCK] for i in range(sums.shape[0] // BLOCK)]
        q = q_ref[:, keys_at].astype(f32) * KEY_CHANNELS ** (-0.5)
        k = k_ref[:, keys_at].astype(f32)
        v = v_ref[:, values_at]
        from_start = jnp.exp(parts[0])
        fine = parts[-1]
        fine3 = fine.reshape(BLOCK // FINE, FINE, KEY_CHANNELS)
        k3 = k.reshape(BLOCK // FINE, FINE, KEY_CHANNELS)
        q3 = q.reshape(BLOCK // FINE, FINE, KEY_CHANNELS)
        terms = []
        for j in range(FINE):
            gap = jnp.minimum(fine3 - fine3[:, j : j + 1, :], 0.0)
            term = q3 * k3[:, j : j + 1, :] * jnp.exp(gap)
            terms.append(term.reshape(BLOCK, KEY_CHANNELS).astype(bf))
        scores = jnp.dot(
            jnp.concatenate(terms, axis=1), spread_ref[...], preferred_element_type=f32
        )
        scores = jnp.where((row // FINE == col // FINE) & (col <= row), scores, 0.0)
        half = BLOCK // 2
        for part in parts[2:-1]:
            near = jnp.exp(part)
            late = row_id % (2 * half) >= half
            q_side = jnp.where(late, q * near, 0.0).astype(bf)
            k_side = jnp.where(late, 0.0, k * near).astype(bf)
            level = lax.dot_general(q_side, k_side, contract_last, preferred_element_type=f32)
            scores += jnp.where(row // (2 * half) == col // (2 * half), level, 0.0)
            half //= 2
        carry = state[h]
        out = lax.dot_general(
            (q * from_start).astype(bf), carry.astype(bf), contract_last, preferred_element_type=f32
        ) + jnp.dot(scores.astype(bf), v, preferred_element_type=f32)
        to_end = (k * jnp.exp(parts[1])).astype(bf)
        state[h] = carry * from_start[BLOCK - 1 :, :] + lax.dot_general(
            v, to_end, (((0,), (0,)), ((), ())), preferred_element_type=f32
        )
        normalized = (
            out * lax.rsqrt(jnp.mean(out * out, axis=-1, keepdims=True) + EPS) * gain_ref[...]
        )
        out_ref[:, values_at] = (own_ref[:, values_at].astype(f32) + normalized).astype(bf)


def attend_kernel(n, heads, steps, n_tp, *refs):
    block_refs, shards, (middle, *full) = refs[:11], refs[11:13], refs[13:16]
    state, produced, out_sem, in_sem, own_sem = refs[16:21]
    held, sems = refs[21:23], refs[23:]
    width = produced.shape[1]
    step = pl.program_id(0)
    ring = Ring(n, shards, held, full, sems)
    ids = [(ring.rep, ring.fs, lax.rem(ring.tp + d, n_tp)) for d in range(1, n_tp)]

    def piece(part, owner):
        rows = pl.ds(pl.multiple_of(part * BLOCK, BLOCK), BLOCK)
        columns = pl.ds(pl.multiple_of(owner * width, KEY_CHANNELS), width)
        return produced.at[rows], middle.at[rows, columns]

    def passing(part, d):
        source, target = piece(part, ring.tp)
        return pltpu.make_async_remote_copy(
            src_ref=source,
            dst_ref=target,
            send_sem=out_sem.at[part, d - 1],
            recv_sem=in_sem.at[part, d - 1],
            device_id=ids[d - 1],
            device_id_type=MESH,
        )

    def keeping(part):
        source, target = piece(part, ring.tp)
        return pltpu.make_async_copy(source, target, own_sem.at[part])

    def hand_out(part):
        for d in range(1, n_tp):
            passing(part, d).start()
        keeping(part).start()

    @pl.when(step == 0)
    def _():
        ring.start(ids)
        state[...] = jnp.zeros_like(state)

    @pl.when(step > 0)
    def _():
        hand_out(step - 1)

    events = ring.events()
    late = [e for i, e in enumerate(events) if (i + 1) * STRIDE >= steps]
    for i, (k, hop) in enumerate(events):
        if (k, hop) not in late:

            @pl.when(step == (i + 1) * STRIDE)
            def _(k=k, hop=hop):
                ring.event(k, hop)

    rows = pl.ds(pl.multiple_of(step * BLOCK, BLOCK), BLOCK)
    attention_block(heads, *block_refs, produced.at[rows], state)

    @pl.when(step == steps - 1)
    def _():
        hand_out(step)
        for k, hop in late:
            ring.event(k, hop)
        ring.finish()

        @pl.loop(0, steps)
        def _(part):
            for d in range(1, n_tp):
                passing(part, d).wait_send()
                _, there = piece(part, lax.rem(ring.tp + n_tp - d, n_tp))
                pltpu.make_async_remote_copy(
                    src_ref=there,
                    dst_ref=there,
                    send_sem=out_sem.at[part, d - 1],
                    recv_sem=in_sem.at[part, d - 1],
                    device_id=ids[d - 1],
                    device_id_type=MESH,
                ).wait_recv()
            keeping(part).wait()


def attend(q, k, v, rate_low, rate_cols, bias_cols, increments, own_cols, head_gain, shards, n, n_tp):
    length, width_qk = q.shape
    heads = width_qk // KEY_CHANNELS
    width_v = v.shape[1]
    steps = length // BLOCK
    sums = jnp.asarray(decay_matrices(), jnp.bfloat16)
    lane = np.arange(FINE * KEY_CHANNELS)[:, None] // KEY_CHANNELS
    spread = jnp.asarray(lane == np.arange(BLOCK)[None, :] % FINE, jnp.bfloat16)

    def rows(width):
        return pl.BlockSpec((BLOCK, width), lambda i: (i, 0))

    def whole(array):
        return pl.BlockSpec(array.shape, lambda i: (0, 0))

    bias_row, gain_row = bias_cols[None], head_gain[None]
    anywhere = pl.BlockSpec(memory_space=pl.ANY)
    peers = max(n_tp - 1, 1)
    return pl.pallas_call(
        functools.partial(attend_kernel, n, heads, steps, n_tp),
        grid=(steps,),
        out_shape=[jax.ShapeDtypeStruct((length, width_v * n_tp), jnp.bfloat16)]
        + gathered_shapes(shards, n),
        in_specs=[
            rows(width_qk),
            rows(width_qk),
            rows(width_v),
            rows(rate_low.shape[1]),
            whole(rate_cols),
            whole(bias_row),
            rows(heads),
            rows(width_v),
            whole(gain_row),
            whole(sums),
            whole(spread),
            anywhere,
            anywhere,
        ],
        out_specs=[anywhere] * 3,
        scratch_shapes=[
            pltpu.VMEM((heads, HEAD_V, KEY_CHANNELS), jnp.float32),
            pltpu.VMEM((length, width_v), jnp.bfloat16),
            pltpu.SemaphoreType.DMA((steps, peers)),
            pltpu.SemaphoreType.DMA((steps, peers)),
            pltpu.SemaphoreType.DMA((steps,)),
        ]
        + ring_scratch(shards, n),
        compiler_params=pltpu.CompilerParams(
            collective_id=2, has_side_effects=True, vmem_limit_bytes=VMEM_LIMIT
        ),
    )(q, k, v, rate_low, rate_cols, bias_row, increments, own_cols, gain_row, sums, spread, *shards)


def feed_kernel(n, n_tp, chunks, middle_ref, gain_ref, up_ref, down_ref, out_ref, *scratch):
    up, down, total, sent, came, load_sem, out_sem, in_sem = scratch
    rep, fs, tp = (lax.axis_index(a) for a in ("rep", "fs", "tp"))
    ids = [(rep, fs, lax.rem(tp + d, n_tp)) for d in range(1, n_tp)]
    step = pl.program_id(0)
    hidden_width = up.shape[1]
    block = down.shape[1]
    width = total.shape[1]
    per_owner = n // n_tp
    loads = (
        pltpu.make_async_copy(up_ref, up, load_sem.at[0]),
        pltpu.make_async_copy(down_ref, down, load_sem.at[1]),
    )

    def passing(part, d):
        rows = pl.ds(pl.multiple_of(part * ROWS, ROWS), ROWS)
        return pltpu.make_async_remote_copy(
            src_ref=sent.at[lax.rem(tp + d, n_tp), rows],
            dst_ref=came.at[tp, rows],
            send_sem=out_sem.at[part, d - 1],
            recv_sem=in_sem.at[part, d - 1],
            device_id=ids[d - 1],
            device_id_type=MESH,
        )

    @pl.when(step == 0)
    def _():
        for load in loads:
            load.start()
        barrier = pltpu.get_barrier_semaphore()
        for device in ids:
            pl.semaphore_signal(barrier, inc=1, device_id=device, device_id_type=MESH)
        pl.semaphore_wait(barrier, n_tp - 1)
        loads[0].wait()

    @pl.when(step > 0)
    def _():
        for d in range(1, n_tp):
            passing(step - 1, d).start()

    rows = pl.ds(pl.multiple_of(step * ROWS, ROWS), ROWS)
    normed = rms_rows(middle_ref[...], gain_ref[...])
    acc = jnp.dot(normed, up[...], preferred_element_type=jnp.float32)
    hidden = jnp.square(jnp.maximum(acc, 0.0)).astype(jnp.bfloat16)

    @pl.when(step == 0)
    def _():
        loads[1].wait()

    for i in range(n):
        term = jnp.dot(
            hidden,
            down[i * hidden_width : (i + 1) * hidden_width, :],
            preferred_element_type=jnp.float32,
        )
        at = (i % per_owner) * block
        sent[i // per_owner, rows, at : at + block] = term.astype(jnp.bfloat16)
    own_at = pl.ds(pl.multiple_of(tp * width, KEY_CHANNELS), width)
    total[rows, :] = middle_ref[:, own_at].astype(jnp.float32) + sent[tp, rows, :].astype(jnp.float32)

    @pl.when(step == chunks - 1)
    def _():
        for d in range(1, n_tp):
            passing(step, d).start()

        @pl.loop(0, chunks)
        def _(part):
            at = pl.ds(pl.multiple_of(part * ROWS, ROWS), ROWS)
            summed = total[at, :]
            for d in range(1, n_tp):
                passing(part, d).wait_send()
                source = lax.rem(tp + n_tp - d, n_tp)
                there = came.at[source, at]
                pltpu.make_async_remote_copy(
                    src_ref=there,
                    dst_ref=there,
                    send_sem=out_sem.at[part, d - 1],
                    recv_sem=in_sem.at[part, d - 1],
                    device_id=ids[d - 1],
                    device_id_type=MESH,
                ).wait_recv()
                summed += came[source, at, :].astype(jnp.float32)
            out_ref[at, :] = summed.astype(jnp.bfloat16)


def feed_forward(middle, gain, up, down, n, n_tp):
    length, features = middle.shape
    width = features // n_tp
    chunks = length // ROWS
    peers = max(n_tp - 1, 1)
    anywhere = pl.BlockSpec(memory_space=pl.ANY)
    return pl.pallas_call(
        functools.partial(feed_kernel, n, n_tp, chunks),
        grid=(chunks,),
        out_shape=jax.ShapeDtypeStruct((length, width), jnp.bfloat16),
        in_specs=[
            pl.BlockSpec((ROWS, features), lambda i: (i, 0)),
            pl.BlockSpec((1, features), lambda i: (0, 0)),
            anywhere,
            anywhere,
        ],
        out_specs=pl.BlockSpec((length, width), lambda i: (0, 0)),
        scratch_shapes=[
            pltpu.VMEM(up.shape, up.dtype),
            pltpu.VMEM(down.shape, down.dtype),
            pltpu.VMEM((length, width), jnp.float32),
            pltpu.VMEM((n_tp, length, width), jnp.bfloat16),
            pltpu.VMEM((n_tp, length, width), jnp.bfloat16),
            pltpu.SemaphoreType.DMA((2,)),
            pltpu.SemaphoreType.DMA((chunks, peers)),
            pltpu.SemaphoreType.DMA((chunks, peers)),
        ],
        compiler_params=pltpu.CompilerParams(
            collective_id=3, has_side_effects=True, vmem_limit_bytes=VMEM_LIMIT
        ),
    )(middle, gain[None], up, down)


def per_device(
    n,
    n_tp,
    resid,
    attention_norm_gain,
    query_weight,
    key_weight,
    value_weight,
    decay_down_weight,
    decay_up_weight,
    decay_rate_bias,
    decay_increment,
    head_norm_gain,
    feedforward_norm_gain,
    up_weight,
    down_weight,
):
    sequence_rows = resid[0]
    col_width = value_weight.shape[1]
    width_qk = query_weight.shape[1]
    own_cols = lax.dynamic_slice_in_dim(sequence_rows, lax.axis_index("tp") * col_width, col_width, 1)
    query_full, key_full, value_full = ring_gather((query_weight, key_weight, value_weight), n, 1)
    normed = rms_rows(sequence_rows, attention_norm_gain)
    q, k, v = (
        jnp.dot(normed, weight, preferred_element_type=jnp.float32).astype(jnp.bfloat16)
        for weight in (query_full, key_full, value_full)
    )
    first_col = lax.axis_index("tp") * width_qk
    rate_cols = lax.dynamic_slice_in_dim(decay_up_weight, first_col, width_qk, 1)
    bias_cols = lax.dynamic_slice_in_dim(decay_rate_bias, first_col, width_qk, 0)
    rate_low = jnp.dot(normed, decay_down_weight, preferred_element_type=jnp.float32).astype(
        jnp.bfloat16
    )
    middle, up_full, down_full = attend(
        q,
        k,
        v,
        rate_low,
        rate_cols,
        bias_cols,
        decay_increment[0],
        own_cols,
        head_norm_gain,
        (up_weight, down_weight),
        n,
        n_tp,
    )
    return feed_forward(middle, feedforward_norm_gain, up_full, down_full, n, n_tp)[None]


def solution(mesh):
    return jax.shard_map(
        functools.partial(per_device, mesh.shape["fs"], mesh.shape["tp"]),
        mesh=mesh,
        in_specs=(
            P(("rep", "fs"), None, None),
            P(),
            P("fs", "tp"),
            P("fs", "tp"),
            P("fs", "tp"),
            P(),
            P(),
            P(),
            P(("rep", "fs"), None, "tp"),
            P(),
            P(),
            P("fs", "tp"),
            P("tp", "fs"),
        ),
        out_specs=P(("rep", "fs"), None, "tp"),
        check_vma=False,
    )
```

time: 763 us -> 222 us (0.29)
  waiting for transfers between devices: 507 us -> 0 us
  Pallas kernels: 0 us -> 192 us
  matrix products: 117 us -> 17 us
  other arithmetic: 83.9 us -> 3.08 us
  local copies, waits for them, and re-layouts: 37.3 us -> 10.2 us
  between operations: 13.7 us -> 0.08 us
    all_gather x6 -> x0, waiting for transfers between devices: 451 us -> none  [the longest x1 125 us: per_device(): down_full = lax.all_gather(down_weight, 'fs', axis=1, tiled=True)]
    pallas_call x0 -> x3, Pallas kernels: none -> 192 us  [the longest x1 87.1 us: attend(): pl.pallas_call(functools.partial(attend_kernel, n, heads, steps, n_tp), g...]
    dot_general x53 -> x4, matrix products: 117 us -> 17 us  [the longest x3 15.7 us: per_device(): jnp.dot(normed, weight, preferred_element_type=jnp.float32)]
    reduce_sum x17 -> x0, other arithmetic: 62.6 us -> none  [the longest x16 59.8 us: block_step(): jnp.sum(q_blk[:, :, None, :] * k_blk[:, None, :, :] * decays, axis=-1)]
    reduce_scatter x1 -> x0, waiting for transfers between devices: 52.7 us -> none  [per_device(): lax.psum_scatter(terms.astype(jnp.bfloat16), 'tp', scatter_dimension=1, t...]
    squeeze x32 -> x0, local copies, waits for them, and re-layouts: 29.7 us -> none  [gated_scan(): lax.scan(block_step, start_state, (split_blocks(queries), split_blocks(ke...]
  transfers between devices with their start and end apart: 7 -> 0, of which waited for: 7 -> 0; matrix products, arithmetic and copies ran while one was open for 4% -> 0% of each run, Pallas kernels for 0% -> 0%
where the time goes in v1:
time: 222 us
  Pallas kernels  192 us (86%)
  matrix products  17 us (8%)
  local copies, waits for them, and re-layouts  10.2 us (5%)
  other arithmetic  3.08 us (1%)
    pallas_call x1, Pallas kernels, attend(): pl.pallas_call(functools.partial(attend_kernel, n, heads, steps, n_tp), g...  87.1 us
    pallas_call x1, Pallas kernels, feed_forward(): pl.pallas_call(functools.partial(feed_kernel, n, n_tp, chunks), grid=(chu...  57.4 us
    pallas_call x1, Pallas kernels, ring_gather(): pl.pallas_call(functools.partial(gather_kernel, n, count), out_shape=gath...  47.2 us
    dot_general x3, matrix products, per_device(): jnp.dot(normed, weight, preferred_element_type=jnp.float32)  15.7 us

profile of v1, /device:TPU:0, one launch (start us, length us, event | category | flops | bytes accessed | tf_op | source)
XLA Modules:
  0.0 222.1 jit_solution(13182556266334925873)
XLA Ops:
  0.0 0.0 copy-start
  0.0 0.0 copy-start.7
  0.0 0.0 copy-start.4
  0.0 0.0 copy-start.1
  0.0 1.5 dynamic_slice.12
  1.5 3.1 %fusion = f32[1024]{0:T(1024)S(1)} fusion(bf16[1,1024,2048]{2,1,0:T(8,128)(2,1)} %param.15), kind=kLoop, calls=%fused_computation.2 | loop fusion | flops 6290432 | bytes 4198400 | tf_op jit(solution)/shard_map/reduce_sum | solution.py:26
  4.6 0.0 copy-done.4
  4.6 0.6 constant_dynamic-slice_fusion.refs_4_
  5.2 0.0 copy-done
  5.2 0.0 copy-done.7
  5.2 0.0 copy-done.1
  5.2 0.0 copy-start.3
  5.2 1.3 convolution_convert_fusion.3
  6.5 0.9 copy.19.refs_3_
  7.4 0.0 copy-done.3
  7.4 1.1 copy.18
  8.4 3.1 %dynamic-slice_bitcast_fusion.refs_7_ = bf16[1024,1024]{1,0:T(8,128)(2,1)} fusion(bf16[1,1024,2048]{2,1,0:T(8,128)(2,1)} %param.15, s32[]{:T(128)S(6)} %select_n.8), kind=kLoop, calls=%fused_computation.5 | loop fusion | bytes 4194308 | tf_op jit(solution)/shard_map/dynamic_slice | solution.py:549
  11.5 47.2 %shard_map.145 = (bf16[2048,512]{1,0:T(8,128)(2,1)}, bf16[2048,512]{1,0:T(8,128)(2,1)}, bf16[2048,1024]{1,0:T(8,128)(2,1)}) custom-call(bf16[256,512]{1,0:T(8,128)(2,1)} %refs_0_.1, bf16[256,512]{1,0:T(8,128)(2,1)} %refs_1_.1, bf16[256,1024]{1,0:T(8,128)(2,1)} %refs_2_.1), custom_call_target="tpu_custom_call" | custom-call | tf_op jit(solution)/shard_map/pallas_call | solution.py:181
  58.7 0.0 copy-start.2
  58.7 0.0 copy-start.6
  58.7 6.4 %convolution_convert_fusion.2.refs_0_ = bf16[1024,512]{1,0:T(8,128)(2,1)} fusion(bf16[2048,512]{1,0:T(8,128)(2,1)} %get-tuple-element.11, bf16[1,1024,2048]{2,1,0:T(8,128)(2,1)} %param.15, f32[2048]{0:T(1024)S(1)} %copy-done.7, f32[1024]{0:T(1024)S(1)} %add_rsqrt_fusion), kind=kOutput, calls=%fused_computation.8 | convolution fusion | flops 2156396544 | bytes 7352320 | tf_op jit(solution)/shard_map/dot_general | solution.py:553
  65.1 0.0 copy-done.2
  65.1 0.0 copy-done.6
  65.1 0.0 copy-start.5
  65.1 3.4 %convolution_convert_fusion.1.refs_1_ = bf16[1024,512]{1,0:T(8,128)(2,1)} fusion(bf16[2048,512]{1,0:T(8,128)(2,1)S(1)} %copy-done.6, bf16[1,1024,2048]{2,1,0:T(8,128)(2,1)S(1)} %copy-done.2, f32[2048]{0:T(1024)S(1)} %copy-done.7, f32[1024]{0:T(1024)S(1)} %add_rsqrt_fusion), kind=kOutput, calls=%fused_computation.7 | convolution fusion | flops 2156396544 | bytes 7352320 | tf_op jit(solution)/shard_map/dot_general | solution.py:553
  68.5 0.0 copy-done.5
  68.5 5.9 %convolution_convert_fusion.refs_2_ = bf16[1024,1024]{1,0:T(8,128)(2,1)} fusion(bf16[2048,1024]{1,0:T(8,128)(2,1)S(1)} %copy-done.5, bf16[1,1024,2048]{2,1,0:T(8,128)(2,1)S(1)} %copy-done.2, f32[2048]{0:T(1024)S(1)} %copy-done.7, f32[1024]{0:T(1024)S(1)} %add_rsqrt_fusion), kind=kOutput, calls=%fused_computation.6 | convolution fusion | flops 4304404480 | bytes 10498048 | tf_op jit(solution)/shard_map/dot_general | solution.py:553
  74.5 87.1 %shard_map.146 = (bf16[1024,2048]{1,0:T(8,128)(2,1)}, bf16[2048,2048]{1,0:T(8,128)(2,1)}, bf16[16384,256]{1,0:T(8,128)(2,1)}) custom-call(bf16[1024,512]{1,0:T(8,128)(2,1)} %convolution_convert_fusion.2.refs_0_, bf16[1024,512]{1,0:T(8,128)(2,1)} %convolution_convert_fusion.1.refs_1_, bf16[1024,1024]{1,0:T(8,128)(2,1)} %convolution_convert_fusion.refs_2_, ...), custom_call_target="tpu_custom_call" | custom-call | tf_op jit(solution)/shard_map/pallas_call | solution.py:376
  161.6 57.4 %shard_map.147 = bf16[1024,1024]{1,0:T(8,128)(2,1)} custom-call(bf16[1024,2048]{1,0:T(8,128)(2,1)} %get-tuple-element.14.middle_ref, f32[1,2048]{1,0:T(1,128)} %bitcast.21, bf16[2048,2048]{1,0:T(8,128)(2,1)} %get-tuple-element.15.up_ref, bf16[16384,256]{1,0:T(8,128)(2,1)} %get-tuple-element.16.down_ref), custom_call_target="tpu_custom_call" | custom-call | tf_op jit(solution)/shard_map/pallas_call | solution.py:502
  219.0 3.1 %copy.21 = bf16[1,1024,1024]{2,1,0:T(8,128)(2,1)} copy(bf16[1,1024,1024]{2,1,0:T(8,128)(2,1)} %bitcast.19) | data formatting | bytes 4194304
  (1 shorter events, 0.0 us)
Async XLA Ops:
  0.0 5.2 %copy-start = (bf16[2048,16]{0,1:T(8,128)(2,1)S(1)}, bf16[2048,16]{0,1:T(8,128)(2,1)}, u32[]{:S(2)}) copy-start(bf16[2048,16]{0,1:T(8,128)(2,1)} %param.20) | copy-start | bytes 196612
  0.0 5.2 %copy-start.7 = (f32[2048]{0:T(1024)S(1)}, f32[2048]{0:T(1024)}, u32[]{:S(2)}) copy-start(f32[2048]{0:T(1024)} %param.16) | copy-start | bytes 24580
  0.0 4.6 %copy-start.4 = (bf16[16,1024]{1,0:T(8,128)(2,1)S(1)}, bf16[16,1024]{1,0:T(8,128)(2,1)}, u32[]{:S(2)}) copy-start(bf16[16,1024]{1,0:T(8,128)(2,1)} %param.21) | copy-start | bytes 98308
  0.0 5.2 %copy-start.1 = (bf16[1,1024,2048]{2,1,0:T(8,128)(2,1)S(1)}, bf16[1,1024,2048]{2,1,0:T(8,128)(2,1)}, u32[]{:S(2)}) copy-start(bf16[1,1024,2048]{2,1,0:T(8,128)(2,1)} %param.15) | copy-start | bytes 12582916
  5.2 2.2 copy-start.3
  58.7 6.4 %copy-start.2 = (bf16[1,1024,2048]{2,1,0:T(8,128)(2,1)S(1)}, bf16[1,1024,2048]{2,1,0:T(8,128)(2,1)}, u32[]{:S(2)}) copy-start(bf16[1,1024,2048]{2,1,0:T(8,128)(2,1)} %param.15) | copy-start | bytes 12582916
  58.7 6.4 %copy-start.6 = (bf16[2048,512]{1,0:T(8,128)(2,1)S(1)}, bf16[2048,512]{1,0:T(8,128)(2,1)}, u32[]{:S(2)}) copy-start(bf16[2048,512]{1,0:T(8,128)(2,1)} %get-tuple-element.12) | copy-start | bytes 6291460
  65.1 3.4 %copy-start.5 = (bf16[2048,1024]{1,0:T(8,128)(2,1)S(1)}, bf16[2048,1024]{1,0:T(8,128)(2,1)}, u32[]{:S(2)}) copy-start(bf16[2048,1024]{1,0:T(8,128)(2,1)} %get-tuple-element.13) | copy-start | bytes 12582916

commit v2 on v1

--- a/solution.py
+++ b/solution.py
@@ -134,26 +134,33 @@
                 self.sending(k, hop + 1, way).start()
             self.twin(k, hop, way).start()
 
+    def twin_arrived(self, k, hop, way):
+        start, half = self.span(k, hop + 1, way)
+        other = start + (1 - 2 * self.rep) * half
+        shift, size = self.cut(half, hop, way)
+        there = self.full[k].at[pl.ds(pl.multiple_of(other + shift, 16), size)]
+        pltpu.make_async_remote_copy(
+            src_ref=there,
+            dst_ref=there,
+            send_sem=self.twin_out.at[k, way, hop],
+            recv_sem=self.twin_in.at[k, way, hop],
+            device_id=self.twin_id,
+            device_id_type=MESH,
+        ).wait_recv()
+
+    def sent(self):
+        for k, hop in self.events():
+            for way in range(2):
+                self.sending(k, hop, way).wait_send()
+                self.twin(k, hop, way).wait_send()
+        for k in range(len(self.held)):
+            self.keep(k).wait()
+
     def finish(self):
         for k, hop in self.events():
             for way in range(2):
-                self.sending(k, hop, way).wait_send()
-                copy = self.twin(k, hop, way)
-                copy.wait_send()
-                start, half = self.span(k, hop + 1, way)
-                other = start + (1 - 2 * self.rep) * half
-                shift, size = self.cut(half, hop, way)
-                there = self.full[k].at[pl.ds(pl.multiple_of(other + shift, 16), size)]
-                pltpu.make_async_remote_copy(
-                    src_ref=there,
-                    dst_ref=there,
-                    send_sem=self.twin_out.at[k, way, hop],
-                    recv_sem=self.twin_in.at[k, way, hop],
-                    device_id=self.twin_id,
-                    device_id_type=MESH,
-                ).wait_recv()
-        for k in range(len(self.held)):
-            self.keep(k).wait()
+                self.twin_arrived(k, hop, way)
+        self.sent()
 
 
 def ring_scratch(shards, n):
@@ -274,13 +281,14 @@
         normalized = (
             out * lax.rsqrt(jnp.mean(out * out, axis=-1, keepdims=True) + EPS) * gain_ref[...]
         )
-        out_ref[:, values_at] = (own_ref[:, values_at].astype(f32) + normalized).astype(bf)
+        own_at = pl.ds(pl.multiple_of(lax.axis_index("tp") * heads * HEAD_V + h * HEAD_V, 128), HEAD_V)
+        out_ref[:, values_at] = (own_ref[:, own_at].astype(f32) + normalized).astype(bf)
 
 
 def attend_kernel(n, heads, steps, n_tp, *refs):
-    block_refs, shards, (middle, *full) = refs[:11], refs[11:13], refs[13:16]
-    state, produced, out_sem, in_sem, own_sem = refs[16:21]
-    held, sems = refs[21:23], refs[23:]
+    block_refs, shards, (middle, *full) = refs[:11], refs[11:12], refs[12:14]
+    state, produced, out_sem, in_sem, own_sem = refs[14:19]
+    held, sems = refs[19:20], refs[20:]
     width = produced.shape[1]
     step = pl.program_id(0)
     ring = Ring(n, shards, held, full, sems)
@@ -386,14 +394,13 @@
             whole(rate_cols),
             whole(bias_row),
             rows(heads),
-            rows(width_v),
+            rows(width_v * n_tp),
             whole(gain_row),
             whole(sums),
             whole(spread),
             anywhere,
-            anywhere,
         ],
-        out_specs=[anywhere] * 3,
+        out_specs=[anywhere] * 2,
         scratch_shapes=[
             pltpu.VMEM((heads, HEAD_V, KEY_CHANNELS), jnp.float32),
             pltpu.VMEM((length, width_v), jnp.bfloat16),
@@ -408,122 +415,138 @@
     )(q, k, v, rate_low, rate_cols, bias_row, increments, own_cols, gain_row, sums, spread, *shards)
 
 
-def feed_kernel(n, n_tp, chunks, middle_ref, gain_ref, up_ref, down_ref, out_ref, *scratch):
-    up, down, total, sent, came, load_sem, out_sem, in_sem = scratch
-    rep, fs, tp = (lax.axis_index(a) for a in ("rep", "fs", "tp"))
-    ids = [(rep, fs, lax.rem(tp + d, n_tp)) for d in range(1, n_tp)]
-    step = pl.program_id(0)
-    hidden_width = up.shape[1]
-    block = down.shape[1]
-    width = total.shape[1]
+def feed_kernel(n, n_tp, middle, gain_ref, up_ref, down_ref, out_ref, down_full, *scratch):
+    up, hidden, block_buf, terms, came, load_sem, block_sem, out_sem, in_sem = scratch[:9]
+    ring = Ring(n, (down_ref,), scratch[9:10], (down_full,), scratch[10:])
+    rep, fs, tp = ring.rep, ring.fs, ring.tp
+    peers = [(rep, fs, lax.rem(tp + d, n_tp)) for d in range(1, n_tp)]
+    length = hidden.shape[0]
+    depth, block = block_buf.shape[1:]
     per_owner = n // n_tp
-    loads = (
-        pltpu.make_async_copy(up_ref, up, load_sem.at[0]),
-        pltpu.make_async_copy(down_ref, down, load_sem.at[1]),
-    )
-
-    def passing(part, d):
-        rows = pl.ds(pl.multiple_of(part * ROWS, ROWS), ROWS)
+    width = per_owner * block
+    load = pltpu.make_async_copy(up_ref, up, load_sem)
+    load.start()
+    ring.start(peers)
+    load.wait()
+
+    def chunk(part):
+        return pl.ds(pl.multiple_of(part * ROWS, ROWS), ROWS)
+
+    @pl.loop(0, length // ROWS)
+    def _(part):
+        normed = rms_rows(middle[chunk(part), :], gain_ref[...])
+        acc = jnp.dot(normed, up[...], preferred_element_type=jnp.float32)
+        hidden[chunk(part), :] = jnp.square(jnp.maximum(acc, 0.0)).astype(jnp.bfloat16)
+
+    def fetch(owner, slot):
+        at = pl.ds(pl.multiple_of(owner * depth, 16), depth)
+        return pltpu.make_async_copy(down_full.at[at], block_buf.at[slot], block_sem.at[slot])
+
+    def multiply(owner, weights):
+        @pl.loop(0, length // (2 * ROWS))
+        def _(part):
+            at = pl.ds(pl.multiple_of(part * 2 * ROWS, ROWS), 2 * ROWS)
+            term = jnp.dot(hidden[at, :], weights[...], preferred_element_type=jnp.float32)
+            terms[owner, at, :] = term.astype(jnp.bfloat16)
+
+    def passing(owner):
+        target = owner // per_owner
         return pltpu.make_async_remote_copy(
-            src_ref=sent.at[lax.rem(tp + d, n_tp), rows],
-            dst_ref=came.at[tp, rows],
-            send_sem=out_sem.at[part, d - 1],
-            recv_sem=in_sem.at[part, d - 1],
-            device_id=ids[d - 1],
+            src_ref=terms.at[owner],
+            dst_ref=came.at[tp, owner - target * per_owner],
+            send_sem=out_sem.at[owner],
+            recv_sem=in_sem.at[tp, owner - target * per_owner],
+            device_id=(rep, fs, target),
             device_id_type=MESH,
         )
 
-    @pl.when(step == 0)
-    def _():
-        for load in loads:
-            load.start()
-        barrier = pltpu.get_barrier_semaphore()
-        for device in ids:
-            pl.semaphore_signal(barrier, inc=1, device_id=device, device_id_type=MESH)
-        pl.semaphore_wait(barrier, n_tp - 1)
-        loads[0].wait()
-
-    @pl.when(step > 0)
-    def _():
+    def hand_out(owner):
+        @pl.when(owner // per_owner != tp)
+        def _():
+            passing(owner).start()
+
+    multiply(fs, ring.held[0])
+    for hop in range(ring.hops):
+        ring.event(0, hop)
+        if hop == 0:
+            hand_out(fs)
+        for way in range(2):
+            ring.twin_arrived(0, hop, way)
+        ways = 2 if hop < ring.hops - 1 else 1
+        owners = [
+            ring_to_fs(lax.rem(ring.me + (n - hop - 1 if way == 0 else hop + 1), n), n)
+            for way in range(ways)
+        ]
+        for way, owner in enumerate(owners):
+            fetch(owner, way).start()
+        for way, owner in enumerate(owners):
+            fetch(owner, way).wait()
+            multiply(owner, block_buf.at[way])
+        for owner in owners:
+            hand_out(owner)
+    ring.sent()
+
+    @pl.loop(0, n)
+    def _(owner):
+        @pl.when(owner // per_owner != tp)
+        def _():
+            passing(owner).wait_send()
+
+    for j in range(per_owner):
         for d in range(1, n_tp):
-            passing(step - 1, d).start()
-
-    rows = pl.ds(pl.multiple_of(step * ROWS, ROWS), ROWS)
-    normed = rms_rows(middle_ref[...], gain_ref[...])
-    acc = jnp.dot(normed, up[...], preferred_element_type=jnp.float32)
-    hidden = jnp.square(jnp.maximum(acc, 0.0)).astype(jnp.bfloat16)
-
-    @pl.when(step == 0)
-    def _():
-        loads[1].wait()
-
-    for i in range(n):
-        term = jnp.dot(
-            hidden,
-            down[i * hidden_width : (i + 1) * hidden_width, :],
-            preferred_element_type=jnp.float32,
-        )
-        at = (i % per_owner) * block
-        sent[i // per_owner, rows, at : at + block] = term.astype(jnp.bfloat16)
+            source = lax.rem(tp + d, n_tp)
+            there = came.at[source, j]
+            pltpu.make_async_remote_copy(
+                src_ref=there,
+                dst_ref=there,
+                send_sem=out_sem.at[j],
+                recv_sem=in_sem.at[source, j],
+                device_id=peers[0],
+                device_id_type=MESH,
+            ).wait_recv()
+
     own_at = pl.ds(pl.multiple_of(tp * width, KEY_CHANNELS), width)
-    total[rows, :] = middle_ref[:, own_at].astype(jnp.float32) + sent[tp, rows, :].astype(jnp.float32)
-
-    @pl.when(step == chunks - 1)
-    def _():
-        for d in range(1, n_tp):
-            passing(step, d).start()
-
-        @pl.loop(0, chunks)
-        def _(part):
-            at = pl.ds(pl.multiple_of(part * ROWS, ROWS), ROWS)
-            summed = total[at, :]
+
+    @pl.loop(0, length // ROWS)
+    def _(part):
+        own = middle[chunk(part), own_at].astype(jnp.float32)
+        for j in range(per_owner):
+            columns = slice(j * block, (j + 1) * block)
+            summed = own[:, columns] + terms[tp * per_owner + j, chunk(part), :].astype(jnp.float32)
             for d in range(1, n_tp):
-                passing(part, d).wait_send()
-                source = lax.rem(tp + n_tp - d, n_tp)
-                there = came.at[source, at]
-                pltpu.make_async_remote_copy(
-                    src_ref=there,
-                    dst_ref=there,
-                    send_sem=out_sem.at[part, d - 1],
-                    recv_sem=in_sem.at[part, d - 1],
-                    device_id=ids[d - 1],
-                    device_id_type=MESH,
-                ).wait_recv()
-                summed += came[source, at, :].astype(jnp.float32)
-            out_ref[at, :] = summed.astype(jnp.bfloat16)
+                source = lax.rem(tp + d, n_tp)
+                summed += came[source, j, chunk(part), :].astype(jnp.float32)
+            out_ref[chunk(part), columns] = summed.astype(jnp.bfloat16)
 
 
 def feed_forward(middle, gain, up, down, n, n_tp):
     length, features = middle.shape
     width = features // n_tp
-    chunks = length // ROWS
-    peers = max(n_tp - 1, 1)
+    depth, block = down.shape
     anywhere = pl.BlockSpec(memory_space=pl.ANY)
+    vmem = pl.BlockSpec(memory_space=pltpu.VMEM)
+    bf = jnp.bfloat16
     return pl.pallas_call(
-        functools.partial(feed_kernel, n, n_tp, chunks),
-        grid=(chunks,),
-        out_shape=jax.ShapeDtypeStruct((length, width), jnp.bfloat16),
-        in_specs=[
-            pl.BlockSpec((ROWS, features), lambda i: (i, 0)),
-            pl.BlockSpec((1, features), lambda i: (0, 0)),
-            anywhere,
-            anywhere,
-        ],
-        out_specs=pl.BlockSpec((length, width), lambda i: (0, 0)),
+        functools.partial(feed_kernel, n, n_tp),
+        out_shape=[jax.ShapeDtypeStruct((length, width), bf)] + gathered_shapes((down,), n),
+        in_specs=[vmem, vmem, anywhere, anywhere],
+        out_specs=[vmem, anywhere],
         scratch_shapes=[
-            pltpu.VMEM(up.shape, up.dtype),
-            pltpu.VMEM(down.shape, down.dtype),
-            pltpu.VMEM((length, width), jnp.float32),
-            pltpu.VMEM((n_tp, length, width), jnp.bfloat16),
-            pltpu.VMEM((n_tp, length, width), jnp.bfloat16),
+            pltpu.VMEM(up.shape, bf),
+            pltpu.VMEM((length, up.shape[1]), bf),
+            pltpu.VMEM((2, depth, block), bf),
+            pltpu.VMEM((n, length, block), bf),
+            pltpu.VMEM((n_tp, n // n_tp, length, block), bf),
+            pltpu.SemaphoreType.DMA,
             pltpu.SemaphoreType.DMA((2,)),
-            pltpu.SemaphoreType.DMA((chunks, peers)),
-            pltpu.SemaphoreType.DMA((chunks, peers)),
-        ],
+            pltpu.SemaphoreType.DMA((n,)),
+            pltpu.SemaphoreType.DMA((n_tp, n // n_tp)),
+        ]
+        + ring_scratch((down,), n),
         compiler_params=pltpu.CompilerParams(
             collective_id=3, has_side_effects=True, vmem_limit_bytes=VMEM_LIMIT
         ),
-    )(middle, gain[None], up, down)
+    )(middle, gain[None], up, down)[0]
 
 
 def per_device(
@@ -544,9 +567,7 @@
     down_weight,
 ):
     sequence_rows = resid[0]
-    col_width = value_weight.shape[1]
     width_qk = query_weight.shape[1]
-    own_cols = lax.dynamic_slice_in_dim(sequence_rows, lax.axis_index("tp") * col_width, col_width, 1)
     query_full, key_full, value_full = ring_gather((query_weight, key_weight, value_weight), n, 1)
     normed = rms_rows(sequence_rows, attention_norm_gain)
     q, k, v = (
@@ -559,7 +580,7 @@
     rate_low = jnp.dot(normed, decay_down_weight, preferred_element_type=jnp.float32).astype(
         jnp.bfloat16
     )
-    middle, up_full, down_full = attend(
+    middle, up_full = attend(
         q,
         k,
         v,
@@ -567,13 +588,13 @@
         rate_cols,
         bias_cols,
         decay_increment[0],
-        own_cols,
+        sequence_rows,
         head_norm_gain,
-        (up_weight, down_weight),
+        (up_weight,),
         n,
         n_tp,
     )
-    return feed_forward(middle, feedforward_norm_gain, up_full, down_full, n, n_tp)[None]
+    return feed_forward(middle, feedforward_norm_gain, up_full, down_weight, n, n_tp)[None]
 
 
 def solution(mesh):

time: 222 us -> 218 us (0.982); the launches traced: 222 us -> 216 us
  local copies, waits for them, and re-layouts: 10.2 us -> 7.15 us
  Pallas kernels: 192 us -> 189 us
    pallas_call x1, Pallas kernels: 87.1 us -> 58.6 us  [attend(): pl.pallas_call(functools.partial(attend_kernel, n, heads, steps, n_tp), g...]
    pallas_call x1, Pallas kernels: 57.4 us -> 82.8 us  [feed_forward(): pl.pallas_call(functools.partial(feed_kernel, n, n_tp), out_shape=[jax.Sh...]
    dynamic_slice x1 -> x0, local copies, waits for them, and re-layouts: 3.09 us -> none  [per_device(): lax.dynamic_slice_in_dim(sequence_rows, lax.axis_index('tp') * col_width,...]
where the time goes in v2:
time: 218 us; the launch traced here: 216 us
  Pallas kernels  189 us (87%)
  matrix products  17 us (8%)
  local copies, waits for them, and re-layouts  7.15 us (3%)
  other arithmetic  3.08 us (1%)
    pallas_call x1, Pallas kernels, feed_forward(): pl.pallas_call(functools.partial(feed_kernel, n, n_tp), out_shape=[jax.Sh...  82.8 us
    pallas_call x1, Pallas kernels, attend(): pl.pallas_call(functools.partial(attend_kernel, n, heads, steps, n_tp), g...  58.6 us
    pallas_call x1, Pallas kernels, ring_gather(): pl.pallas_call(functools.partial(gather_kernel, n, count), out_shape=gath...  47.2 us
    dot_general x3, matrix products, per_device(): jnp.dot(normed, weight, preferred_element_type=jnp.float32)  15.7 us

profile of v2, /device:TPU:0, one launch (start us, length us, event | category | flops | bytes accessed | tf_op | source)
XLA Modules:
  0.0 215.8 jit_solution(5921615430688999158)
XLA Ops:
  0.0 0.0 copy-start
  0.0 0.0 copy-start.7
  0.0 0.0 copy-start.4
  0.0 0.0 copy-start.1
  0.0 1.5 dynamic_slice.7
  1.5 3.1 %fusion = f32[1024]{0:T(1024)S(1)} fusion(bf16[1,1024,2048]{2,1,0:T(8,128)(2,1)} %param.15), kind=kLoop, calls=%fused_computation.2 | loop fusion | flops 6290432 | bytes 4198400 | tf_op jit(solution)/shard_map/reduce_sum | solution.py:26
  4.6 0.0 copy-done.4
  4.6 0.6 constant_dynamic-slice_fusion.refs_4_
  5.2 0.0 copy-done
  5.2 0.0 copy-done.7
  5.2 0.0 copy-done.1
  5.2 0.0 copy-start.3
  5.2 1.3 convolution_convert_fusion.3
  6.5 0.9 copy.19.refs_3_
  7.4 0.0 copy-done.3
  7.4 1.1 copy.18
  8.4 47.2 %shard_map.145 = (bf16[2048,512]{1,0:T(8,128)(2,1)}, bf16[2048,512]{1,0:T(8,128)(2,1)}, bf16[2048,1024]{1,0:T(8,128)(2,1)}) custom-call(bf16[256,512]{1,0:T(8,128)(2,1)} %refs_0_.1, bf16[256,512]{1,0:T(8,128)(2,1)} %refs_1_.1, bf16[256,1024]{1,0:T(8,128)(2,1)} %refs_2_.1), custom_call_target="tpu_custom_call" | custom-call | tf_op jit(solution)/shard_map/pallas_call | solution.py:188
  55.6 0.0 copy-start.2
  55.6 0.0 copy-start.6
  55.6 6.4 %convolution_convert_fusion.2.refs_0_ = bf16[1024,512]{1,0:T(8,128)(2,1)} fusion(bf16[2048,512]{1,0:T(8,128)(2,1)} %get-tuple-element.11, f32[2048]{0:T(1024)S(1)} %copy-done.7, f32[1024]{0:T(1024)S(1)} %add_rsqrt_fusion, bf16[1,1024,2048]{2,1,0:T(8,128)(2,1)} %param.15), kind=kOutput, calls=%fused_computation.7 | convolution fusion | flops 2156396544 | bytes 7352320 | tf_op jit(solution)/shard_map/dot_general | solution.py:574
  62.1 0.0 copy-done.2
  62.1 0.0 copy-done.6
  62.1 0.0 copy-start.5
  62.1 3.3 %convolution_convert_fusion.1.refs_1_ = bf16[1024,512]{1,0:T(8,128)(2,1)} fusion(bf16[2048,512]{1,0:T(8,128)(2,1)S(1)} %copy-done.6, f32[2048]{0:T(1024)S(1)} %copy-done.7, f32[1024]{0:T(1024)S(1)} %add_rsqrt_fusion, bf16[1,1024,2048]{2,1,0:T(8,128)(2,1)S(1)} %copy-done.2), kind=kOutput, calls=%fused_computation.6 | convolution fusion | flops 2156396544 | bytes 7352320 | tf_op jit(solution)/shard_map/dot_general | solution.py:574
  65.4 0.0 copy-done.5
  65.4 6.0 %convolution_convert_fusion.refs_2_ = bf16[1024,1024]{1,0:T(8,128)(2,1)} fusion(bf16[2048,1024]{1,0:T(8,128)(2,1)S(1)} %copy-done.5, f32[2048]{0:T(1024)S(1)} %copy-done.7, f32[1024]{0:T(1024)S(1)} %add_rsqrt_fusion, bf16[1,1024,2048]{2,1,0:T(8,128)(2,1)S(1)} %copy-done.2), kind=kOutput, calls=%fused_computation.5 | convolution fusion | flops 4304404480 | bytes 10498048 | tf_op jit(solution)/shard_map/dot_general | solution.py:574
  71.4 58.6 %shard_map.146 = (bf16[1024,2048]{1,0:T(8,128)(2,1)}, bf16[2048,2048]{1,0:T(8,128)(2,1)}) custom-call(bf16[1024,512]{1,0:T(8,128)(2,1)} %convolution_convert_fusion.2.refs_0_, bf16[1024,512]{1,0:T(8,128)(2,1)} %convolution_convert_fusion.1.refs_1_, bf16[1024,1024]{1,0:T(8,128)(2,1)} %convolution_convert_fusion.refs_2_, bf16[1024,16]{1,0:T(8,128)(2,1)} %copy.19.refs_3_, ...), custom_call_target="tpu_custom_call" | custom-call | tf_op jit(solution)/shard_map/pallas_call | solution.py:384
  130.0 82.8 %shard_map.147 = (bf16[1024,1024]{1,0:T(8,128)(2,1)}, bf16[16384,256]{1,0:T(8,128)(2,1)}) custom-call(bf16[1024,2048]{1,0:T(8,128)(2,1)} %get-tuple-element.14.middle, f32[1,2048]{1,0:T(1,128)} %bitcast.19, bf16[2048,2048]{1,0:T(8,128)(2,1)} %get-tuple-element.15.up_ref, bf16[2048,256]{1,0:T(8,128)(2,1)} %down_ref.1), custom_call_target="tpu_custom_call" | custom-call | tf_op jit(solution)/shard_map/pallas_call | solution.py:529
  212.8 3.1 %copy.21 = bf16[1,1024,1024]{2,1,0:T(8,128)(2,1)} copy(bf16[1,1024,1024]{2,1,0:T(8,128)(2,1)} %bitcast.18) | data formatting | bytes 4194304
  (1 shorter events, 0.0 us)
Async XLA Ops:
  0.0 5.2 %copy-start = (bf16[2048,16]{0,1:T(8,128)(2,1)S(1)}, bf16[2048,16]{0,1:T(8,128)(2,1)}, u32[]{:S(2)}) copy-start(bf16[2048,16]{0,1:T(8,128)(2,1)} %param.20) | copy-start | bytes 196612
  0.0 5.2 %copy-start.7 = (f32[2048]{0:T(1024)S(1)}, f32[2048]{0:T(1024)}, u32[]{:S(2)}) copy-start(f32[2048]{0:T(1024)} %param.16) | copy-start | bytes 24580
  0.0 4.6 %copy-start.4 = (bf16[16,1024]{1,0:T(8,128)(2,1)S(1)}, bf16[16,1024]{1,0:T(8,128)(2,1)}, u32[]{:S(2)}) copy-start(bf16[16,1024]{1,0:T(8,128)(2,1)} %param.21) | copy-start | bytes 98308
  0.0 5.2 %copy-start.1 = (bf16[1,1024,2048]{2,1,0:T(8,128)(2,1)S(1)}, bf16[1,1024,2048]{2,1,0:T(8,128)(2,1)}, u32[]{:S(2)}) copy-start(bf16[1,1024,2048]{2,1,0:T(8,128)(2,1)} %param.15) | copy-start | bytes 12582916
  5.2 2.1 copy-start.3
  55.6 6.5 %copy-start.2 = (bf16[1,1024,2048]{2,1,0:T(8,128)(2,1)S(1)}, bf16[1,1024,2048]{2,1,0:T(8,128)(2,1)}, u32[]{:S(2)}) copy-start(bf16[1,1024,2048]{2,1,0:T(8,128)(2,1)} %param.15) | copy-start | bytes 12582916
  55.6 6.5 %copy-start.6 = (bf16[2048,512]{1,0:T(8,128)(2,1)S(1)}, bf16[2048,512]{1,0:T(8,128)(2,1)}, u32[]{:S(2)}) copy-start(bf16[2048,512]{1,0:T(8,128)(2,1)} %get-tuple-element.12) | copy-start | bytes 6291460
  62.1 3.4 %copy-start.5 = (bf16[2048,1024]{1,0:T(8,128)(2,1)S(1)}, bf16[2048,1024]{1,0:T(8,128)(2,1)}, u32[]{:S(2)}) copy-start(bf16[2048,1024]{1,0:T(8,128)(2,1)} %get-tuple-element.13) | copy-start | bytes 12582916
